TPU v7x, 256 devices: a whole 4x4x8 slice. The times are simulated.
256 devices in a mesh: sp: 16 (over y, x), dp: 16 (over z, core).
Axes of the slice: x: 4, y: 4, z: 8, core: 2. Of those that a mesh axis runs over, the one named last changes fastest.
Arguments:
- tokens: bfloat16 [16, 2048, 2048], P('dp', 'sp'), may hold values from -6 to 6
- query_weight: bfloat16 [2048, 1024], P('dp'), may hold values from -0.125 to 0.125
- key_weight: bfloat16 [2048, 1024], P('dp'), may hold values from -0.125 to 0.125
- value_weight: bfloat16 [2048, 2048], P('dp'), may hold values from -0.125 to 0.125
- output_weight: bfloat16 [2048, 2048], P('dp'), may hold values from -0.125 to 0.125
- log_decay: float32 [2, 16], P(None, 'sp'), may hold values from -0.04 to 0, as said below
Outputs:
- mixed: bfloat16 [16, 2048, 2048], P('dp', 'sp')
Inputs may be any that keep to these rules, and one draw needn't show every extreme that they name: `log_decay`: every entry is negative: the logarithm of a head's decay per position.
All inputs are finite; a program needn't handle non-finite values.
Results may differ from a plain program's by a relative error of at most 0.012.
Values may be sent and summed in bfloat16 or wider, within the bound.
No kernel may reach another device: no remote copies, remote signals or barrier semaphores. Data moves between devices by JAX's collectives and lax.ppermute only.
A program may use at most 128 MiB of HBM per device.

v0:
```python
import jax
import jax.numpy as jnp
from jax import lax
from jax.sharding import PartitionSpec as P

HEADS = 16
DK = 64
DV = 128
BLOCK = 512


def in_order(pieces, dim):
    lengths = list(pieces.shape[1:])
    lengths[dim] *= pieces.shape[0]
    return jnp.moveaxis(pieces, 0, dim).reshape(lengths)


def copy_for_each(shard, axis):
    count = lax.axis_size(axis)
    return lax.all_to_all(
        jnp.broadcast_to(shard[None], (count, *shard.shape)), axis, 0, 0, tiled=True
    )


def gathered_copies(shard, axis, dim):
    return in_order(copy_for_each(shard, axis), dim)


def rotate(values_part, positions):
    half_dim = values_part.shape[-1] // 2
    frequency = 10000.0 ** (-jnp.arange(half_dim, dtype=jnp.float32) / half_dim)
    angles = positions[:, None] * frequency[None, :]
    cosine = jnp.cos(angles)[:, None, :]
    sine_part = jnp.sin(angles)[:, None, :]
    first = values_part[..., :half_dim]
    second = values_part[..., half_dim:]
    return jnp.concatenate(
        [first * cosine - second * sine_part, first * sine_part + second * cosine], axis=-1
    )


def retain(query, key_rows, value_rows, log_rate):
    length, heads, key_dim = query.shape
    value_dim = value_rows.shape[-1]
    count = length // BLOCK
    offsets = jnp.arange(BLOCK, dtype=jnp.float32)
    distance = offsets[:, None] - offsets[None, :]
    decay_inner = jnp.where(
        distance[None] >= 0.0,
        jnp.exp(log_rate[:, None, None] * jnp.maximum(distance, 0.0)[None]),
        0.0,
    )
    decay_query = jnp.exp((offsets[:, None] + 1.0) * log_rate[None, :])[:, :, None]
    decay_key = jnp.exp((BLOCK - 1.0 - offsets)[:, None] * log_rate[None, :])[:, :, None]
    decay_block = jnp.exp(BLOCK * log_rate)[:, None, None]

    def blocks(array):
        return array.reshape(count, BLOCK, heads, array.shape[-1])

    def advance(state, inputs):
        query_block, key_block, value_block = inputs
        inner = (
            jnp.einsum("ihd,jhd->hij", query_block, key_block, preferred_element_type=jnp.float32)
            * decay_inner
        )
        result = jnp.einsum(
            "hij,jhv->ihv",
            inner.astype(jnp.bfloat16),
            value_block,
            preferred_element_type=jnp.float32,
        )
        query_wide = query_block.astype(jnp.float32) * decay_query
        result = result + jnp.einsum("ihd,hdv->ihv", query_wide, state)
        key_wide = key_block.astype(jnp.float32) * decay_key
        state = state * decay_block + jnp.einsum(
            "jhd,jhv->hdv", key_wide, value_block.astype(jnp.float32)
        )
        return (state, result)

    initial = jnp.zeros((heads, key_dim, value_dim), jnp.float32)
    final_state, outputs = lax.scan(
        advance, initial, (blocks(query), blocks(key_rows), blocks(value_rows))
    )
    return outputs.reshape(length, heads, value_dim)


def mechanism(stacked, log_decay):
    length = stacked.shape[0]
    widened = stacked[..., : 2 * DK].astype(jnp.float32)
    positions = jnp.arange(length, dtype=jnp.float32)
    query = rotate(widened[..., :DK], positions).astype(jnp.bfloat16)
    key_rows = rotate(widened[..., DK : 2 * DK], positions).astype(jnp.bfloat16)
    value_rows = stacked[..., 2 * DK :]
    forward = retain(query, key_rows, value_rows, log_decay[0])
    backward = retain(
        jnp.flip(query, 0), jnp.flip(key_rows, 0), jnp.flip(value_rows, 0), log_decay[1]
    )
    combined = forward + jnp.flip(backward, 0)
    average = jnp.mean(combined, axis=-1, keepdims=True)
    centred = combined - average
    variance = jnp.mean(centred * centred, axis=-1, keepdims=True)
    return (centred * lax.rsqrt(variance + 1e-06)).astype(jnp.bfloat16)


def shards(tokens, query_weight, key_weight, value_weight, output_weight, log_decay):
    rows = tokens[0]
    row_count = rows.shape[0]
    local_heads = log_decay.shape[1]
    first_head = lax.axis_index("sp") * local_heads
    own_slices = jnp.concatenate(
        [
            lax.dynamic_slice_in_dim(query_weight, first_head * DK, local_heads * DK, 1),
            lax.dynamic_slice_in_dim(key_weight, first_head * DK, local_heads * DK, 1),
            lax.dynamic_slice_in_dim(value_weight, first_head * DV, local_heads * DV, 1),
        ],
        axis=1,
    )
    own_whole = gathered_copies(own_slices, "dp", 0)
    piece = lax.all_gather(rows, "sp", axis=0, tiled=True)
    count = piece.shape[0]
    product = jnp.dot(piece, own_whole, preferred_element_type=jnp.float32).astype(jnp.bfloat16)
    query_part = product[:, : local_heads * DK].reshape(count, local_heads, DK)
    key_part = product[:, local_heads * DK : 2 * local_heads * DK].reshape(count, local_heads, DK)
    value_part = product[:, 2 * local_heads * DK :].reshape(count, local_heads, DV)
    gathered = jnp.concatenate([query_part, key_part, value_part], axis=2)
    normed = mechanism(gathered, log_decay)
    by_token = lax.all_to_all(normed, "sp", split_axis=0, concat_axis=1, tiled=True).reshape(
        row_count, HEADS * DV
    )
    mixed = jnp.dot(
        by_token,
        lax.all_gather(output_weight, "dp", axis=0, tiled=True),
        preferred_element_type=jnp.float32,
    )
    return mixed.astype(jnp.bfloat16)[None]


def solution(mesh):
    placed = (
        P("dp", "sp", None),
        P("dp", None),
        P("dp", None),
        P("dp", None),
        P("dp", None),
        P(None, "sp"),
    )
    return jax.shard_map(
        shards, mesh=mesh, in_specs=placed, out_specs=P("dp", "sp", None), check_vma=False
    )
```

profile of v0, /device:TPU:32, one launch (start us, length us, event | category | flops | bytes accessed | tf_op | source)
XLA Modules:
  0.0 171.1 jit_solution(11749039148471384118)
XLA Ops:
  10.1 8.6 %all-to-all-start = ((bf16[16,128,256]{2,1,0:T(8,128)(2,1)}), bf16[16,128,256]{2,1,0:T(8,128)(2,1)S(1)}, u32[]{:S(2)}, u32[]{:S(2)}) async-start(bf16[16,128,256]{2,1,0:T(8,128)(2,1)} %broadcast_in_dim.18), calls=%async_computation | async-start | bytes 2097152 | tf_op jit(solution)/shard_map/all_to_all | solution.py:20
  18.7 1.4 fusion.116
  21.5 21.8 %all-to-all-done = bf16[16,128,256]{2,1,0:T(8,128)(2,1)S(1)} async-done(((bf16[16,128,256]{2,1,0:T(8,128)(2,1)}), bf16[16,128,256]{2,1,0:T(8,128)(2,1)S(1)}, u32[]{:S(2)}, u32[]{:S(2)}) %all-to-all-start) | async-done | bytes 1048608 | tf_op jit(solution)/shard_map/all_to_all | solution.py:20
  43.3 45.0 %all-gather.6.cloned.1.call-done = bf16[1,2048,2048]{2,1,0:T(8,128)(2,1)} async-done(((bf16[1,128,2048]{2,1,0:T(8,128)(2,1)}), bf16[1,2048,2048]{2,1,0:T(8,128)(2,1)}) %all-gather.6.cloned.1.call-update) | async-done | bytes 8388624 | tf_op jit(solution)/shard_map/all_gather | solution.py:119
  88.3 5.8 %fusion.109 = bf16[2048,256]{0,1:T(8,128)(2,1)S(1)} fusion(bf16[2048,256]{1,0:T(8,128)(2,1)S(1)} %bitcast.255, bf16[1,2048,2048]{2,1,0:T(8,128)(2,1)} %all-gather.6.cloned.1.call-done), kind=kOutput, calls=%fused_computation.103 | convolution fusion | flops 2148007936 | bytes 10485760 | tf_op jit(solution)/shard_map/dot_general | solution.py:121
  95.1 1.6 reverse.3
  96.9 1.2 subtract_convert_fusion
  98.3 1.4 rev.14
  99.7 1.4 rev.13
  102.2 17.2 %while.31 = (s32[]{:T(128)}, f32[1,64,128]{2,1,0:T(8,128)S(1)}, f32[4,512,1,128]{3,1,0,2:T(8,128)S(1)}, f32[1,1,1]{2,1,0:T(1,128)}, bf16[4,512,1,64]{1,3,2,0:T(8...) while((s32[]{:T(128)}, f32[1,64,128]{2,1,0:T(8,128)S(1)}, ...), condition=%wide.region_3.4_spmd.clone.clone.clone, body=%wide.region_2.3_spmd.clone.clone.clone.sunk | while | flops 119506944 | bytes 2469500 | solution.py:81
  102.2 2.2 %fusion.158 = f32[128,512]{1,0:T(8,128)S(1)} fusion(f32[]{:T(128)} %get-tuple-element.508, bf16[4,512,1,128]{3,1,2,0:T(8,128)(2,1)S(1)} %get-tuple-element.506, s32[]{:T(128)} %get-tuple-element.491, bf16[4,512,1,64]{1,3,2,0:T(8,128)(2,1)S(1)} %get-tuple-element.507, bf16[4,512,1,64]{1,3,2,0:T(8,128)(2,1)} %get-tuple-element.505), kind=kOutput, calls=%fused_computation.55.clone.1 | convolution fusion | flops 102498304 | bytes 526336 | tf_op jit(solution)/shard_map/while/body/eval_jaxpr/hij,jhv->ihv/dot_general | solution.py:66
  106.5 2.2 %fusion.158 = f32[128,512]{1,0:T(8,128)S(1)} fusion(f32[]{:T(128)} %get-tuple-element.508, bf16[4,512,1,128]{3,1,2,0:T(8,128)(2,1)S(1)} %get-tuple-element.506, s32[]{:T(128)} %get-tuple-element.491, bf16[4,512,1,64]{1,3,2,0:T(8,128)(2,1)S(1)} %get-tuple-element.507, bf16[4,512,1,64]{1,3,2,0:T(8,128)(2,1)} %get-tuple-element.505), kind=kOutput, calls=%fused_computation.55.clone.1 | convolution fusion | flops 102498304 | bytes 526336 | tf_op jit(solution)/shard_map/while/body/eval_jaxpr/hij,jhv->ihv/dot_general | solution.py:66
  110.9 2.2 %fusion.158 = f32[128,512]{1,0:T(8,128)S(1)} fusion(f32[]{:T(128)} %get-tuple-element.508, bf16[4,512,1,128]{3,1,2,0:T(8,128)(2,1)S(1)} %get-tuple-element.506, s32[]{:T(128)} %get-tuple-element.491, bf16[4,512,1,64]{1,3,2,0:T(8,128)(2,1)S(1)} %get-tuple-element.507, bf16[4,512,1,64]{1,3,2,0:T(8,128)(2,1)} %get-tuple-element.505), kind=kOutput, calls=%fused_computation.55.clone.1 | convolution fusion | flops 102498304 | bytes 526336 | tf_op jit(solution)/shard_map/while/body/eval_jaxpr/hij,jhv->ihv/dot_general | solution.py:66
  115.2 2.2 %fusion.158 = f32[128,512]{1,0:T(8,128)S(1)} fusion(f32[]{:T(128)} %get-tuple-element.508, bf16[4,512,1,128]{3,1,2,0:T(8,128)(2,1)S(1)} %get-tuple-element.506, s32[]{:T(128)} %get-tuple-element.491, bf16[4,512,1,64]{1,3,2,0:T(8,128)(2,1)S(1)} %get-tuple-element.507, bf16[4,512,1,64]{1,3,2,0:T(8,128)(2,1)} %get-tuple-element.505), kind=kOutput, calls=%fused_computation.55.clone.1 | convolution fusion | flops 102498304 | bytes 526336 | tf_op jit(solution)/shard_map/while/body/eval_jaxpr/hij,jhv->ihv/dot_general | solution.py:66
  120.7 17.5 %while.30 = (s32[]{:T(128)}, f32[1,64,128]{2,1,0:T(8,128)S(1)}, f32[4,512,1,128]{3,1,0,2:T(8,128)S(1)}, f32[1,1,1]{2,1,0:T(1,128)}, bf16[4,512,1,64]{1,3,2,0:T(8...) while((s32[]{:T(128)}, f32[1,64,128]{2,1,0:T(8,128)S(1)}, ...), condition=%wide.region_1.2_spmd.clone.clone.clone, body=%wide.region_0.1_spmd.clone.clone.clone.sunk | while | flops 119506944 | bytes 2469500 | solution.py:81
  120.7 2.2 %fusion.148 = f32[128,512]{1,0:T(8,128)S(1)} fusion(f32[]{:T(128)} %get-tuple-element.538, bf16[4,512,1,128]{3,1,2,0:T(8,128)(2,1)} %get-tuple-element.536, s32[]{:T(128)} %get-tuple-element.521, bf16[4,512,1,64]{1,3,2,0:T(8,128)(2,1)S(1)} %get-tuple-element.537, bf16[4,512,1,64]{1,3,2,0:T(8,128)(2,1)} %get-tuple-element.535), kind=kOutput, calls=%fused_computation.8.clone.1 | convolution fusion | flops 102498304 | bytes 526336 | tf_op jit(solution)/shard_map/while/body/eval_jaxpr/hij,jhv->ihv/dot_general | solution.py:66
  124.0 1.1 fusion.147
  125.1 2.2 %fusion.148 = f32[128,512]{1,0:T(8,128)S(1)} fusion(f32[]{:T(128)} %get-tuple-element.538, bf16[4,512,1,128]{3,1,2,0:T(8,128)(2,1)} %get-tuple-element.536, s32[]{:T(128)} %get-tuple-element.521, bf16[4,512,1,64]{1,3,2,0:T(8,128)(2,1)S(1)} %get-tuple-element.537, bf16[4,512,1,64]{1,3,2,0:T(8,128)(2,1)} %get-tuple-element.535), kind=kOutput, calls=%fused_computation.8.clone.1 | convolution fusion | flops 102498304 | bytes 526336 | tf_op jit(solution)/shard_map/while/body/eval_jaxpr/hij,jhv->ihv/dot_general | solution.py:66
  128.3 1.1 fusion.147
  129.4 2.2 %fusion.148 = f32[128,512]{1,0:T(8,128)S(1)} fusion(f32[]{:T(128)} %get-tuple-element.538, bf16[4,512,1,128]{3,1,2,0:T(8,128)(2,1)} %get-tuple-element.536, s32[]{:T(128)} %get-tuple-element.521, bf16[4,512,1,64]{1,3,2,0:T(8,128)(2,1)S(1)} %get-tuple-element.537, bf16[4,512,1,64]{1,3,2,0:T(8,128)(2,1)} %get-tuple-element.535), kind=kOutput, calls=%fused_computation.8.clone.1 | convolution fusion | flops 102498304 | bytes 526336 | tf_op jit(solution)/shard_map/while/body/eval_jaxpr/hij,jhv->ihv/dot_general | solution.py:66
  132.7 1.1 fusion.147
  133.8 2.2 %fusion.148 = f32[128,512]{1,0:T(8,128)S(1)} fusion(f32[]{:T(128)} %get-tuple-element.538, bf16[4,512,1,128]{3,1,2,0:T(8,128)(2,1)} %get-tuple-element.536, s32[]{:T(128)} %get-tuple-element.521, bf16[4,512,1,64]{1,3,2,0:T(8,128)(2,1)S(1)} %get-tuple-element.537, bf16[4,512,1,64]{1,3,2,0:T(8,128)(2,1)} %get-tuple-element.535), kind=kOutput, calls=%fused_computation.8.clone.1 | convolution fusion | flops 102498304 | bytes 526336 | tf_op jit(solution)/shard_map/while/body/eval_jaxpr/hij,jhv->ihv/dot_general | solution.py:66
  141.5 16.4 %all_to_all.20 = bf16[16,2,8192]{2,1,0:T(2,128)(2,1)S(1)} all-to-all(bf16[16,2,8192]{2,1,0:T(2,128)(2,1)S(1)} %reshape.742), channel_id=1, replica_groups=mesh['sp'=16,'dp'=16] {'sp'}, dimensions={0} | all-to-all | bytes 1048576 | tf_op jit(solution)/shard_map/all_to_all | solution.py:127
  158.8 5.5 %fusion.112 = bf16[1,128,2048]{2,1,0:T(8,128)(2,1)} fusion(bf16[128,2048]{0,1:T(8,128)(2,1)S(1)} %bitcast.246, bf16[2048,2048]{1,0:T(8,128)(2,1)} %all-gather.4.cloned.1.call-done), kind=kOutput, calls=%fused_computation.105 | convolution fusion | flops 1074003968 | bytes 9437184 | tf_op jit(solution)/shard_map/dot_general | solution.py:130
  (80 shorter events, 24.7 us)
Async XLA Ops:
  6.5 1.5 copy-start
  6.5 81.7 %all-gather.6.cloned.1.call-start = ((), (), s32[]{:S(2)}) async-start(), calls=%async_computation.3 | async-start | bytes 8912896 | tf_op jit(solution)/shard_map/all_gather | solution.py:119
  7.3 151.5 %all-gather.4.cloned.1.call-start = ((), (), s32[]{:S(2)}) async-start(), calls=%async_computation.2 | async-start | bytes 8912896 | tf_op jit(solution)/shard_map/all_gather | solution.py:132
  10.1 33.2 %all-to-all-start = ((bf16[16,128,256]{2,1,0:T(8,128)(2,1)}), bf16[16,128,256]{2,1,0:T(8,128)(2,1)S(1)}, u32[]{:S(2)}, u32[]{:S(2)}) async-start(bf16[16,128,256]{2,1,0:T(8,128)(2,1)} %broadcast_in_dim.18), calls=%async_computation | async-start | bytes 2097152 | tf_op jit(solution)/shard_map/all_to_all | solution.py:20
Sparse Core Ops, SparseCore 0:
  9.8 78.4 all-gather.5
  90.1 53.8 all-gather.3
where the time goes:
time: 172 us; the launch traced here: 171 us
  waiting for transfers between devices  68.2 us (40%)
  matrix products  39 us (23%)
  blocking collectives  16.4 us (10%)
  between operations  15 us (9%)
  local copies, waits for them, and re-layouts  13.2 us (8%)
  other arithmetic  10.2 us (6%)
  starting transfers between devices  8.63 us (5%)
    all_gather x1, waiting for transfers between devices, shards(): piece = lax.all_gather(rows, 'sp', axis=0, tiled=True)  45 us
    all_to_all x1, waiting for transfers between devices, copy_for_each(): lax.all_to_all(jnp.broadcast_to(shard[None], (count, *shard.shape)), axis...  21.8 us
    dot_general x8, matrix products, advance(): jnp.einsum('hij,jhv->ihv', inner.astype(jnp.bfloat16), value_block, prefe...  17.5 us
    all_to_all x1, blocking collectives, shards(): lax.all_to_all(normed, 'sp', split_axis=0, concat_axis=1, tiled=True)  16.4 us
    all_to_all x1, starting transfers between devices, copy_for_each(): lax.all_to_all(jnp.broadcast_to(shard[None], (count, *shard.shape)), axis...  8.59 us
    dot_general x8, matrix products, advance(): jnp.einsum('jhd,jhv->hdv', key_wide, value_block.astype(jnp.float32))  8.43 us
    dot_general x1, matrix products, shards(): jnp.dot(piece, own_whole, preferred_element_type=jnp.float32)  5.77 us
    dot_general x1, matrix products, shards(): jnp.dot(by_token, lax.all_gather(output_weight, 'dp', axis=0, tiled=True)...  5.47 us
  transfers between devices with their start and end apart: 3, of which 2 were waited for; matrix products, arithmetic and copies ran while one was open for 33% of the time, Pallas kernels for 0%

commit v1 on v0

--- a/solution.py
+++ b/solution.py
@@ -116,7 +116,10 @@
         axis=1,
     )
     own_whole = gathered_copies(own_slices, "dp", 0)
-    piece = lax.all_gather(rows, "sp", axis=0, tiled=True)
+    dev_n = lax.psum(1, "sp")
+    kept_rows = [dev_n if i0 == 0 else 1 for i0 in range(rows.ndim)]
+    t1 = jnp.tile(rows, kept_rows)
+    piece = lax.all_to_all(t1, axis_name="sp", split_axis=0, concat_axis=0, tiled=True)
     count = piece.shape[0]
     product = jnp.dot(piece, own_whole, preferred_element_type=jnp.float32).astype(jnp.bfloat16)
     query_part = product[:, : local_heads * DK].reshape(count, local_heads, DK)

time: 172 us -> 270 us (1.57); the launches traced: 171 us -> 265 us
  waiting for transfers between devices: 68.2 us -> 124 us
  blocking collectives: 16.4 us -> 48.5 us
  local copies, waits for them, and re-layouts: 13.2 us -> 19.1 us
    all_to_all x1, waiting for transfers between devices: 21.8 us -> 124 us  [shards(): lax.all_to_all(t1, axis_name='sp', split_axis=0, concat_axis=0, tiled=True)]
    all_gather x1 -> x0, waiting for transfers between devices: 45 us -> none  [shards(): piece = lax.all_gather(rows, 'sp', axis=0, tiled=True)]
    all_to_all x0 -> x1, blocking collectives: none -> 33.8 us  [copy_for_each(): lax.all_to_all(jnp.broadcast_to(shard[None], (count, *shard.shape)), axis...]
    another operation x3 -> x4, local copies, waits for them, and re-layouts: 1.78 us -> 7.11 us  [the longest x1 5.33 us: shards(): t1 = jnp.tile(rows, kept_rows)]
  transfers between devices with their start and end apart: 3 -> 2, of which waited for: 2 -> 1; matrix products, arithmetic and copies ran while one was open for 33% -> 21% of each run, Pallas kernels for 0% -> 0%
where the time goes in v1:
time: 270 us; the launch traced here: 265 us
  waiting for transfers between devices  124 us (46%)
  blocking collectives  48.5 us (18%)
  matrix products  38.8 us (14%)
  local copies, waits for them, and re-layouts  19.1 us (7%)
  between operations  15 us (6%)
  other arithmetic  11.8 us (4%)
  starting transfers between devices  7.26 us (3%)
    all_to_all x1, waiting for transfers between devices, shards(): lax.all_to_all(t1, axis_name='sp', split_axis=0, concat_axis=0, tiled=True)  124 us
    all_to_all x1, blocking collectives, copy_for_each(): lax.all_to_all(jnp.broadcast_to(shard[None], (count, *shard.shape)), axis...  33.8 us
    dot_general x8, matrix products, advance(): jnp.einsum('hij,jhv->ihv', inner.astype(jnp.bfloat16), value_block, prefe...  17.3 us
    all_to_all x1, blocking collectives, shards(): lax.all_to_all(normed, 'sp', split_axis=0, concat_axis=1, tiled=True)  14.7 us
    dot_general x8, matrix products, advance(): jnp.einsum('jhd,jhv->hdv', key_wide, value_block.astype(jnp.float32))  8.42 us
    all_to_all x1, starting transfers between devices, shards(): lax.all_to_all(t1, axis_name='sp', split_axis=0, concat_axis=0, tiled=True)  7.22 us
    dot_general x1, matrix products, shards(): jnp.dot(piece, own_whole, preferred_element_type=jnp.float32)  5.77 us
    dot_general x1, matrix products, shards(): jnp.dot(by_token, lax.all_gather(output_weight, 'dp', axis=0, tiled=True)...  5.46 us
  transfers between devices with their start and end apart: 2, of which 1 were waited for; matrix products, arithmetic and copies ran while one was open for 21% of the time, Pallas kernels for 0%

profile of v1, /device:TPU:32, one launch (start us, length us, event | category | flops | bytes accessed | tf_op | source)
XLA Modules:
  0.0 265.3 jit_solution(2221008132712319299)
XLA Ops:
  8.7 33.8 %all_to_all.29 = bf16[16,128,256]{2,1,0:T(8,128)(2,1)S(1)} all-to-all(bf16[16,128,256]{2,1,0:T(8,128)(2,1)S(1)} %broadcast_in_dim.18), channel_id=1, replica_groups=mesh['sp'=16,'dp'=16] {'dp'}, dimensions={0} | all-to-all | bytes 2097152 | tf_op jit(solution)/shard_map/all_to_all | solution.py:20
  42.5 5.3 %tile.9 = bf16[16,128,2048]{2,1,0:T(8,128)(2,1)} broadcast(bf16[128,2048]{1,0:T(8,128)(2,1)} %bitcast.254), dimensions={1,2} | broadcast | bytes 8912896 | tf_op jit(solution)/shard_map/tile | solution.py:121
  47.8 7.2 %all-to-all-start.1 = ((bf16[16,128,2048]{2,1,0:T(8,128)(2,1)}), bf16[16,128,2048]{2,1,0:T(8,128)(2,1)}, u32[]{:S(2)}, u32[]{:S(2)}) async-start(bf16[16,128,2048]{2,1,0:T(8,128)(2,1)} %tile.9), calls=%async_computation.1 | async-start | bytes 16777216 | tf_op jit(solution)/shard_map/all_to_all | solution.py:122
  57.8 123.8 %all-to-all-done.1 = bf16[16,128,2048]{2,1,0:T(8,128)(2,1)} async-done(((bf16[16,128,2048]{2,1,0:T(8,128)(2,1)}), bf16[16,128,2048]{2,1,0:T(8,128)(2,1)}, u32[]{:S(2)}, u32[]{:S(2)}) %all-to-all-start.1) | async-done | bytes 8388640 | tf_op jit(solution)/shard_map/all_to_all | solution.py:122
  181.6 5.8 %fusion.104 = bf16[2048,256]{0,1:T(8,128)(2,1)S(1)} fusion(bf16[2048,256]{1,0:T(8,128)(2,1)S(1)} %bitcast.251, bf16[2048,2048]{1,0:T(8,128)(2,1)} %bitcast.3), kind=kOutput, calls=%fused_computation.101 | convolution fusion | flops 2148007936 | bytes 10485760 | tf_op jit(solution)/shard_map/dot_general | solution.py:124
  188.4 1.6 reverse.3
  190.2 1.2 subtract_convert_fusion
  192.9 1.4 rev.14
  194.3 1.4 rev.13
  196.8 16.8 %while.31 = (s32[]{:T(128)}, f32[1,64,128]{2,1,0:T(8,128)S(1)}, f32[4,512,1,128]{3,1,0,2:T(8,128)S(1)}, f32[1,1,1]{2,1,0:T(1,128)}, bf16[4,512,1,64]{1,3,2,0:T(8...) while((s32[]{:T(128)}, f32[1,64,128]{2,1,0:T(8,128)S(1)}, ...), condition=%wide.region_3.4_spmd.clone.clone.clone, body=%wide.region_2.3_spmd.clone.clone.clone.sunk | while | flops 119506944 | bytes 2469500 | solution.py:81
  196.8 2.1 fusion.152
  201.0 2.1 fusion.152
  205.2 2.1 fusion.152
  209.4 2.1 fusion.152
  214.9 1.7 pad_maximum_fusion
  216.7 17.5 %while.30 = (s32[]{:T(128)}, f32[1,64,128]{2,1,0:T(8,128)S(1)}, f32[4,512,1,128]{3,1,0,2:T(8,128)S(1)}, f32[1,1,1]{2,1,0:T(1,128)}, bf16[4,512,1,64]{1,3,2,0:T(8...) while((s32[]{:T(128)}, f32[1,64,128]{2,1,0:T(8,128)S(1)}, ...), condition=%wide.region_1.2_spmd.clone.clone.clone, body=%wide.region_0.1_spmd.clone.clone.clone.sunk | while | flops 119506944 | bytes 2469500 | solution.py:81
  216.7 2.2 fusion.142
  219.9 1.1 fusion.141
  221.0 2.2 fusion.142
  225.4 2.2 fusion.142
  228.6 1.1 fusion.141
  229.8 2.2 fusion.142
  237.4 14.7 %all_to_all.30 = bf16[16,2,8192]{2,1,0:T(2,128)(2,1)S(1)} all-to-all(bf16[16,2,8192]{2,1,0:T(2,128)(2,1)S(1)} %reshape.748), channel_id=1, replica_groups=mesh['sp'=16,'dp'=16] {'sp'}, dimensions={0} | all-to-all | bytes 1048576 | tf_op jit(solution)/shard_map/all_to_all | solution.py:130
  253.0 5.5 %fusion.105 = bf16[1,128,2048]{2,1,0:T(8,128)(2,1)} fusion(bf16[128,2048]{0,1:T(8,128)(2,1)S(1)} %bitcast.242, bf16[2048,2048]{1,0:T(8,128)(2,1)} %all-gather.2.cloned.1.call-done), kind=kOutput, calls=%fused_computation.103 | convolution fusion | flops 1074003968 | bytes 9437184 | tf_op jit(solution)/shard_map/dot_general | solution.py:133
  (81 shorter events, 27.0 us)
Async XLA Ops:
  6.5 1.0 copy-start
  47.8 8.0 %copy-start.1 = (f32[2,1]{0,1:T(1,128)S(1)}, f32[2,1]{0,1:T(1,128)}, u32[]{:S(2)}) copy-start(f32[2,1]{0,1:T(1,128)} %param.15) | copy-start | bytes 28
  47.8 133.7 %all-to-all-start.1 = ((bf16[16,128,2048]{2,1,0:T(8,128)(2,1)}), bf16[16,128,2048]{2,1,0:T(8,128)(2,1)}, u32[]{:S(2)}, u32[]{:S(2)}) async-start(bf16[16,128,2048]{2,1,0:T(8,128)(2,1)} %tile.9), calls=%async_computation.1 | async-start | bytes 16777216 | tf_op jit(solution)/shard_map/all_to_all | solution.py:122
  55.1 197.9 %all-gather.2.cloned.1.call-start = ((), (), s32[]{:S(2)}) async-start(), calls=%async_computation.3 | async-start | bytes 8912896 | tf_op jit(solution)/shard_map/all_gather | solution.py:135
Sparse Core Ops, SparseCore 0:
  57.7 54.1 all-gather.1
